TPU v7x, 32 devices: a whole 2x2x4 slice. The times are simulated.
32 devices in a mesh: sp: 4 (over z), fs: 4 (over y, x), tp: 2 (over core).
Axes of the slice: x: 2, y: 2, z: 4, core: 2. Of those that a mesh axis runs over, the one named last changes fastest.
Arguments:
- tokens: bfloat16 [4, 1024, 2048], P('fs', 'sp', 'tp'), may hold values from -6 to 6
- norm_gain: float32 [2048], replicated, may hold values from 0.1 to 1.9
- ret_query: bfloat16 [2048, 1024], P('sp', 'tp'), may hold values from -0.125 to 0.125
- ret_key: bfloat16 [2048, 1024], P('sp', 'tp'), may hold values from -0.125 to 0.125
- ret_value: bfloat16 [2048, 1024], P('sp', 'tp'), may hold values from -0.125 to 0.125
- att_query: bfloat16 [2048, 1024], P('sp', 'tp'), may hold values from -0.125 to 0.125
- att_key: bfloat16 [2048, 256], P('sp', 'tp'), may hold values from -0.125 to 0.125
- att_value: bfloat16 [2048, 256], P('sp', 'tp'), may hold values from -0.125 to 0.125
- log_decay: float32 [4, 4, 1024], P('fs', 'tp', 'sp'), may hold values from -1 to 0
- start_state: float32 [4, 4, 256, 256], P('fs', 'tp'), may hold values from -12 to 12
- ret_gain: float32 [1024], P('tp'), may hold values from 0.1 to 1.9
- sink_logits: float32 [16], P('tp'), may hold values from 1 to 5
- ret_out: bfloat16 [1024, 2048], P('tp', 'fs'), may hold values from -0.1875 to 0.1875
- att_out: bfloat16 [1024, 2048], P('tp', 'fs'), may hold values from -1.5 to 1.5
Outputs:
- mixed: bfloat16 [4, 1024, 2048], P('fs', 'sp', 'tp')
All inputs are finite; a program needn't handle non-finite values.
Results may differ from a plain program's by a relative error of at most 0.015.
Values may be sent and summed in bfloat16 or wider, within the bound.
A program may use at most 128 MiB of HBM per device.

v0:
```python
import jax
import jax.numpy as jnp
from jax import lax
from jax.sharding import PartitionSpec as P

DK = 256
DV = 256
HD = 64
WINDOW = 128
BLOCK = 128
epsilon = 1e-06
exact_result = lax.Precision.HIGHEST


def carried_in(array, axis, combine, identity):
    peers, mine = (lax.axis_size(axis), lax.axis_index(axis))
    everything = jax.tree.map(
        lambda part, kind: lax.all_gather(part.astype(kind), axis),
        array,
        (jnp.bfloat16, jnp.bfloat16),
    )
    start = jax.tree.map(
        lambda part, zero: jnp.broadcast_to(jnp.asarray(zero, part.dtype), part.shape),
        array,
        identity,
    )

    def hop(k, before):
        reached = k < mine
        new = combine(
            before, jax.tree.map(lambda part, own: part[k].astype(own.dtype), everything, array)
        )
        return jax.tree.map(lambda a, b: jnp.where(reached, a, b), new, before)

    return lax.fori_loop(0, peers, hop, start)


def passed_along(block, axis, distance):
    devices = range(lax.axis_size(axis))
    route = [(i - distance, i) for i in devices if i - distance in devices]
    return lax.ppermute(block, axis, route)


def rotate(values, positions):
    half_dim = values.shape[-1] // 2
    inverse = 1.0 / 10000.0 ** (jnp.arange(half_dim, dtype=jnp.float32) / half_dim)
    angles = positions.astype(jnp.float32)[:, None] * inverse[None, :]
    cosine = jnp.cos(angles)[:, None, :]
    sine_table = jnp.sin(angles)[:, None, :]
    front_half = values[..., :half_dim]
    back_half = values[..., half_dim:]
    return jnp.concatenate(
        [
            front_half * cosine - back_half * sine_table,
            front_half * sine_table + back_half * cosine,
        ],
        axis=-1,
    )


def block_step(memory_state, inputs):
    queries, key_matrix_rows, value_matrix_rows, log_rates = inputs
    length_here = log_rates.shape[-1]
    causal = jnp.arange(length_here)[:, None] >= jnp.arange(length_here)[None, :]
    running_totals = jnp.cumsum(log_rates, axis=-1)
    relative = running_totals[:, :, None] - running_totals[:, None, :]
    weight = jnp.where(causal[None], jnp.exp(jnp.where(causal[None], relative, 0.0)), 0.0)
    score_matrix = (
        jnp.einsum("hqd,hkd->hqk", queries, key_matrix_rows, precision=exact_result) * weight
    )
    carried_state = jnp.einsum(
        "hqd,hdv->hqv",
        queries * jnp.exp(running_totals)[:, :, None],
        memory_state,
        precision=exact_result,
    )
    output_rows = (
        jnp.einsum("arf,afu->aru", score_matrix, value_matrix_rows, precision=exact_result)
        + carried_state
    )
    decay_factors = jnp.exp(running_totals[:, -1:] - running_totals)
    memory_state = memory_state * jnp.exp(running_totals[:, -1])[:, None, None] + jnp.einsum(
        "iwj,iwe->ije",
        key_matrix_rows * decay_factors[:, :, None],
        value_matrix_rows,
        precision=exact_result,
    )
    return (memory_state, output_rows)


def chain(earlier, later):
    return (earlier[0] * later[0], earlier[1] * later[0][:, None, None] + later[1])


def shards(
    tokens,
    norm_gain,
    ret_query,
    ret_key,
    ret_value,
    att_query,
    att_key,
    att_value,
    log_decay,
    start_state,
    ret_gain,
    sink_logits,
    ret_out,
    att_out,
):
    gathered = lax.all_gather(tokens[0], "tp", axis=1, tiled=True)
    row_count = gathered.shape[0]
    as_float = gathered.astype(jnp.float32)
    normed = (
        as_float
        * lax.rsqrt(jnp.mean(as_float * as_float, axis=-1, keepdims=True) + epsilon)
        * norm_gain
    ).astype(jnp.bfloat16)
    offset = lax.axis_index("sp") * row_count
    positions = offset + jnp.arange(row_count, dtype=jnp.int32)
    weights = (ret_query, ret_key, ret_value, att_query, att_key, att_value)
    pieces = (
        lax.all_gather(weights[0], "sp", axis=0, tiled=True),
        lax.all_gather(weights[1], "sp", axis=0, tiled=True),
        lax.all_gather(weights[2], "sp", axis=0, tiled=True),
        lax.all_gather(weights[3], "sp", axis=0, tiled=True),
        lax.all_gather(weights[4], "sp", axis=0, tiled=True),
        lax.all_gather(weights[5], "sp", axis=0, tiled=True),
    )
    projected = tuple(
        (jnp.dot(normed, piece, preferred_element_type=jnp.float32) for piece in pieces)
    )
    rounded = tuple((product_f.astype(jnp.bfloat16) for product_f in projected))
    projected = rounded[:3]
    head_count = projected[0].shape[1] // DK
    queries = rotate(projected[0].astype(jnp.float32).reshape(row_count, head_count, DK), positions)
    keys_rot = rotate(
        projected[1].astype(jnp.float32).reshape(row_count, head_count, DK), positions
    ) * DK ** (-0.5)
    values_f = projected[2].astype(jnp.float32).reshape(row_count, head_count, DV)
    log_rates = log_decay[0]
    count = row_count // BLOCK

    def blocked(array):
        return array.reshape(count, BLOCK, head_count, array.shape[-1]).transpose(0, 2, 1, 3)

    rates_blocked = log_rates.reshape(head_count, count, BLOCK).transpose(1, 0, 2)
    local_state, pieces = lax.scan(
        block_step,
        jnp.zeros((head_count, DK, DV), jnp.float32),
        (blocked(queries), blocked(keys_rot), blocked(values_f), rates_blocked),
    )
    local_out = pieces.transpose(0, 2, 1, 3).reshape(row_count, head_count, DV)
    running_totals = jnp.cumsum(log_rates, axis=-1)
    device_decay = jnp.exp(running_totals[:, -1])
    identity = (jnp.ones((head_count,), jnp.float32), jnp.zeros((head_count, DK, DV), jnp.float32))
    prior_decay, prior_state = carried_in((device_decay, local_state), "sp", chain, identity)
    incoming = prior_state + prior_decay[:, None, None] * start_state[0]
    retained = local_out + jnp.einsum(
        "thd,hdv->thv",
        queries * jnp.exp(running_totals).T[:, :, None],
        incoming,
        precision=exact_result,
    )
    centred = retained - jnp.mean(retained, axis=-1, keepdims=True)
    variance = jnp.mean(centred * centred, axis=-1, keepdims=True)
    ret_hidden = (
        (centred * lax.rsqrt(variance + epsilon)).reshape(row_count, head_count * DV) * ret_gain
    ).astype(jnp.bfloat16)
    att_queries, att_keys, att_values = rounded[3:]
    kv_heads = att_keys.shape[1] // HD
    groups = att_queries.shape[1] // HD // kv_heads
    earlier_keys, earlier_values = passed_along(
        (att_keys[row_count - WINDOW :], att_values[row_count - WINDOW :]), "sp", 1
    )
    extended_keys = jnp.concatenate([earlier_keys, att_keys], axis=0)
    extended_values = jnp.concatenate([earlier_values, att_values], axis=0)
    windows = row_count // WINDOW

    def banded(array):
        earlier = array[:row_count].reshape(windows, WINDOW, kv_heads, HD)
        current = array[WINDOW:].reshape(windows, WINDOW, kv_heads, HD)
        return jnp.concatenate([earlier, current], axis=1)

    key_band = banded(extended_keys)
    value_band = banded(extended_values)
    grouped_q = att_queries.reshape(windows, WINDOW, kv_heads, groups, HD)
    score_matrix = jnp.einsum(
        "nqhgd,nkhd->nhgqk", grouped_q, key_band, preferred_element_type=jnp.float32
    ) * HD ** (-0.5)
    query_index = WINDOW + jnp.arange(WINDOW)
    key_index = jnp.arange(2 * WINDOW)
    allowed = (key_index[None, :] <= query_index[:, None]) & (
        query_index[:, None] - key_index[None, :] < WINDOW
    )
    key_place = offset - WINDOW + jnp.arange(windows)[:, None] * WINDOW + key_index[None, :]
    visible = (allowed[None] & (key_place >= 0)[:, None, :])[:, None, None]
    expo = jnp.exp(jnp.where(visible, score_matrix, -1e30))
    summed = jnp.sum(expo, axis=-1, keepdims=True) + jnp.exp(sink_logits).reshape(
        1, kv_heads, groups, 1, 1
    )
    probs = (expo / summed).astype(jnp.bfloat16)
    attended = jnp.einsum(
        "nhgqk,nkhd->nqhgd", probs, value_band, preferred_element_type=jnp.float32
    )
    att_hidden = attended.astype(jnp.bfloat16).reshape(row_count, kv_heads * groups * HD)
    ret_width = ret_hidden.shape[1]
    joined = jnp.concatenate([ret_hidden, att_hidden], axis=1)[None]
    piece = lax.all_gather(joined, "fs", axis=0, tiled=True)
    product = jnp.einsum(
        "srh,hd->srd", piece[:, :, :ret_width], ret_out, preferred_element_type=jnp.float32
    )
    product = product + jnp.einsum(
        "srh,hd->srd", piece[:, :, ret_width:], att_out, preferred_element_type=jnp.float32
    )
    partial_rows = product.astype(jnp.bfloat16)
    regrouped = lax.all_to_all(partial_rows, "fs", split_axis=0, concat_axis=2, tiled=True)
    mixed = lax.psum_scatter(
        regrouped[0].astype(jnp.float32).astype(jnp.bfloat16), "tp", scatter_dimension=1, tiled=True
    )
    return mixed[None]


def solution(mesh):
    placed = (
        P("fs", "sp", "tp"),
        P(),
        P("sp", "tp"),
        P("sp", "tp"),
        P("sp", "tp"),
        P("sp", "tp"),
        P("sp", "tp"),
        P("sp", "tp"),
        P("fs", "tp", "sp"),
        P("fs", "tp", None, None),
        P("tp"),
        P("tp"),
        P("tp", "fs"),
        P("tp", "fs"),
    )
    return jax.shard_map(
        shards, mesh=mesh, in_specs=placed, out_specs=P("fs", "sp", "tp"), check_vma=False
    )
```

profile of v0, /device:TPU:0, one launch (start us, length us, event | category | flops | bytes accessed | tf_op | source)
XLA Modules:
  0.0 330.0 jit_solution(6295431087866726067)
XLA Ops:
  6.6 0.7 all-gather.20.cloned.1.call-update
  7.3 0.7 all-gather.12.cloned.1.call-update
  8.1 0.7 all-gather.16.cloned.1.call-update
  13.0 13.6 %all-reduce = bf16[8]{0:T(256)(128)(2,1)S(1)} all-reduce(bf16[8]{0:T(256)(128)(2,1)S(1)} %dynamic-update-slice), channel_id=3, replica_groups=mesh['sp'=4,'fs'=4,'tp'=2] {'sp'}, use_global_device_ids=true, to_apply=%add | all-reduce | flops 8 | bytes 32
  26.6 18.4 %all_gather.42 = bf16[2048,128]{1,0:T(8,128)(2,1)S(1)} all-gather(bf16[512,128]{1,0:T(8,128)(2,1)S(1)} %copy-done.12), channel_id=1, replica_groups=mesh['sp'=4,'fs'=4,'tp'=2] {'sp'}, dimensions={0}, use_global_device_ids=true | all-gather | bytes 655360 | tf_op jit(solution)/shard_map/all_gather | solution.py:127
  45.7 21.2 %all_gather.41 = bf16[2048,128]{1,0:T(8,128)(2,1)} all-gather(bf16[512,128]{1,0:T(8,128)(2,1)S(1)} %copy-done.13), channel_id=1, replica_groups=mesh['sp'=4,'fs'=4,'tp'=2] {'sp'}, dimensions={0}, use_global_device_ids=true | all-gather | bytes 655360 | tf_op jit(solution)/shard_map/all_gather | solution.py:128
  66.9 1.2 multiply_cosine_fusion
  68.1 0.8 broadcast_and_fusion
  68.9 1.6 fusion.25
  70.5 1.7 convolution_convert_fusion.5
  72.9 2.6 collective-permute-start.1
  75.5 5.5 %all-gather.12.cloned.1.call-done = bf16[2048,512]{1,0:T(8,128)(2,1)} async-done(((bf16[512,512]{1,0:T(8,128)(2,1)}), bf16[2048,512]{1,0:T(8,128)(2,1)}) %all-gather.12.cloned.1.call-update) | async-done | bytes 2097168 | tf_op jit(solution)/shard_map/all_gather | solution.py:124
  80.9 2.3 fusion.31
  83.6 44.0 %all-gather.16.cloned.1.call-done = bf16[2048,512]{1,0:T(8,128)(2,1)} async-done(((bf16[512,512]{1,0:T(8,128)(2,1)}), bf16[2048,512]{1,0:T(8,128)(2,1)}) %all-gather.16.cloned.1.call-update) | async-done | bytes 2097168 | tf_op jit(solution)/shard_map/all_gather | solution.py:123
  127.6 2.7 fusion.33
  130.3 1.1 reshape.299
  131.4 42.1 %all-gather.14.cloned.1.call-done = bf16[2048,512]{1,0:T(8,128)(2,1)} async-done(((bf16[512,512]{1,0:T(8,128)(2,1)}), bf16[2048,512]{1,0:T(8,128)(2,1)}) %all-gather.14.cloned.1.call-update) | async-done | bytes 2097168 | tf_op jit(solution)/shard_map/all_gather | solution.py:125
  173.6 2.7 fusion.32
  176.6 1.3 fusion.65
  178.9 6.7 %while.29 = (s32[]{:T(128)}, f32[2,256,256]{2,1,0:T(8,128)S(1)}, f32[2,2,128,256]{3,2,1,0:T(8,128)}, f32[2,2,128]{2,1,0:T(2,128)S(1)}, f32[2,2,128,256]{3,2,0,1:...) while((s32[]{:T(128)}, f32[2,256,256]{2,1,0:T(8,128)S(1)}, ...), condition=%wide.region_3.4_spmd.clone, body=%wide.region_1.3_spmd.clone.sunk | while | flops 604880896 | bytes 4242084 | solution.py:148
  180.2 1.2 fusion.95
  181.4 0.8 convolution_add_fusion.3
  183.6 1.2 fusion.95
  184.8 0.8 convolution_add_fusion.3
  185.6 0.7 convert_element_type.102
  186.4 1.9 convolution_convert_fusion.6
  188.6 2.3 collective-permute-start
  191.0 0.8 pad_maximum_fusion.2
  192.0 1.0 collective-permute-done
  193.2 1.3 copy.65
  194.9 24.5 %all-gather.18.cloned.1.call-done = bf16[2048,512]{1,0:T(8,128)(2,1)} async-done(((bf16[512,512]{1,0:T(8,128)(2,1)}), bf16[2048,512]{1,0:T(8,128)(2,1)}) %all-gather.18.cloned.1.call-update) | async-done | bytes 2097168 | tf_op jit(solution)/shard_map/all_gather | solution.py:126
  219.5 2.3 convolution_convert_fusion.1
  223.8 25.1 %all-gather.22.cloned.1.call-done = bf16[8,256,256]{2,1,0:T(8,128)(2,1)} async-done(((bf16[2,256,256]{2,1,0:T(8,128)(2,1)}), bf16[8,256,256]{2,1,0:T(8,128)(2,1)}) %all-gather.22.cloned.1.call-update) | async-done | bytes 1048592 | tf_op jit(solution)/shard_map/all_gather | solution.py:18
  248.9 4.6 %while.30 = (s32[]{:T(128)}, f32[2]{0:T(128)S(1)}, f32[2,256,256]{2,1,0:T(8,128)S(1)}, s32[]{:T(128)}, bf16[4,2]{1,0:T(4,128)(2,1)S(1)}, /*index=5*/bf16[4,2,256,256]{3,2,1,0:T(8,128)(2,1)}, s32[]{:T(128)}, s32[]{:T(128)}) while((s32[]{:T(128)}, f32[2]{0:T(128)S(1)}, f32[2,256,256]{2,1,0:T(8,128)S(1)}, s32[]{:T(128)}, ...), condition=%wide.region_7.8_spmd.clone, body=%wide.region_6.7_spmd.clone.sunk | while | flops 655372 | bytes 1310871 | solution.py:35
  248.9 1.2 fusion.96
  250.1 1.1 fusion.96
  251.3 1.1 fusion.96
  252.4 1.1 fusion.96
  253.6 1.2 fusion.67
  255.0 0.8 pad_maximum_fusion.1
  255.9 34.5 %all-gather.24.cloned.1.call-done = bf16[1024,1024]{0,1:T(8,128)(2,1)} async-done(((bf16[256,1024]{0,1:T(8,128)(2,1)}), bf16[1024,1024]{0,1:T(8,128)(2,1)}) %all-gather.24.cloned.1.call-update) | async-done | bytes 2097168 | tf_op jit(solution)/shard_map/all_gather | solution.py:209
  290.4 2.9 copy.81
  293.3 0.7 fusion.36
  294.4 0.7 add_convert_fusion
  295.1 16.7 %all_to_all.15 = bf16[4,256,512]{2,1,0:T(8,128)(2,1)S(1)} all-to-all(bf16[4,256,512]{2,1,0:T(8,128)(2,1)S(1)} %add_convert_fusion), channel_id=1, replica_groups=mesh['sp'=4,'fs'=4,'tp'=2] {'fs'}, dimensions={0} | all-to-all | bytes 2097152 | tf_op jit(solution)/shard_map/all_to_all | solution.py:217
  311.8 1.3 copy.82
  313.1 8.0 %reduce-scatter.2.cloned.1.call-done = bf16[256,1024]{0,1:T(8,128)(2,1)} async-done(((bf16[256,2048]{0,1:T(8,128)(2,1)}), bf16[256,1024]{0,1:T(8,128)(2,1)}) %reduce-scatter.2.cloned.1.call-update) | async-done | bytes 524304 | tf_op jit(solution)/shard_map/reduce_scatter | solution.py:218
  321.1 2.0 copy.83
  (138 shorter events, 13.2 us)
Async XLA Ops:
  6.5 286.8 %copy-start = (bf16[512,512]{1,0:T(8,128)(2,1)S(1)}, bf16[512,512]{1,0:T(8,128)(2,1)}, u32[]{:S(2)}) copy-start(bf16[512,512]{1,0:T(8,128)(2,1)} %param.30) | copy-start | bytes 1572868
  6.5 4.8 %copy-start.23 = (u32[32]{0:T(128)S(1)}, u32[32]{0:T(128)}, u32[]{:S(2)}) copy-start(u32[32]{0:T(128)} %constant.93) | copy-start | bytes 388
  6.5 3.5 %copy-start.15 = (f32[1,2,256]{2,1,0:T(2,128)S(1)}, f32[1,2,256]{2,1,0:T(2,128)}, u32[]{:S(2)}) copy-start(f32[1,2,256]{2,1,0:T(2,128)} %param.26) | copy-start | bytes 6148
  6.5 20.1 %copy-start.12 = (bf16[512,128]{1,0:T(8,128)(2,1)S(1)}, bf16[512,128]{1,0:T(8,128)(2,1)}, u32[]{:S(2)}) copy-start(bf16[512,128]{1,0:T(8,128)(2,1)} %param.24) | copy-start | bytes 393220
  6.5 38.6 %copy-start.22 = (f32[8]{0:T(128)S(1)}, f32[8]{0:T(128)}, u32[]{:S(2)}) copy-start(f32[8]{0:T(128)} %param.29) | copy-start | bytes 100
  6.5 39.2 %copy-start.13 = (bf16[512,128]{1,0:T(8,128)(2,1)S(1)}, bf16[512,128]{1,0:T(8,128)(2,1)}, u32[]{:S(2)}) copy-start(bf16[512,128]{1,0:T(8,128)(2,1)} %param.25) | copy-start | bytes 393220
  6.6 62.3 %all-gather.20.cloned.1.call-start = ((), (), s32[]{:S(2)}) async-start(), calls=%async_computation.7 | async-start | bytes 1572864 | tf_op jit(solution)/shard_map/all_gather | solution.py:111
  7.3 73.6 %all-gather.12.cloned.1.call-start = ((), (), s32[]{:S(2)}) async-start(), calls=%async_computation.2 | async-start | bytes 2621440 | tf_op jit(solution)/shard_map/all_gather | solution.py:124
  8.0 62.5 %copy-start.20 = (f32[2048]{0:T(1024)S(1)}, f32[2048]{0:T(1024)}, u32[]{:S(2)}) copy-start(f32[2048]{0:T(1024)} %param.19) | copy-start | bytes 24580
  8.1 119.6 %all-gather.16.cloned.1.call-start = ((), (), s32[]{:S(2)}) async-start(), calls=%async_computation.4 | async-start | bytes 2621440 | tf_op jit(solution)/shard_map/all_gather | solution.py:123
  8.8 164.8 %all-gather.14.cloned.1.call-start = ((), (), s32[]{:S(2)}) async-start(), calls=%async_computation.3 | async-start | bytes 2621440 | tf_op jit(solution)/shard_map/all_gather | solution.py:125
  9.4 210.1 %all-gather.18.cloned.1.call-start = ((), (), s32[]{:S(2)}) async-start(), calls=%async_computation.5 | async-start | bytes 2621440 | tf_op jit(solution)/shard_map/all_gather | solution.py:126
  10.0 238.9 %all-gather.22.cloned.1.call-start = ((), (), s32[]{:S(2)}) async-start(), calls=%async_computation.8 | async-start | bytes 1310720 | tf_op jit(solution)/shard_map/all_gather | solution.py:18
  68.9 12.1 %copy-start.5 = (bf16[1,256,2048]{2,1,0:T(8,128)(2,1)S(1)}, bf16[1,256,2048]{2,1,0:T(8,128)(2,1)}, u32[]{:S(2)}) copy-start(bf16[1,256,2048]{2,1,0:T(8,128)(2,1)} %all-gather.20.cloned.1.call-done) | copy-start | bytes 3145732
  70.5 103.1 %copy-start.18 = (f32[256]{0:T(256)}, f32[256]{0:T(256)S(1)}, u32[]{:S(2)}) copy-start(f32[256]{0:T(256)S(1)} %add_rsqrt_fusion.1) | copy-start | bytes 3076
  72.2 11.0 %copy-start.10 = (bf16[256,128]{1,0:T(8,128)(2,1)}, bf16[256,128]{1,0:T(8,128)(2,1)S(1)}, u32[]{:S(2)}) copy-start(bf16[256,128]{1,0:T(8,128)(2,1)S(1)} %convolution_convert_fusion.5) | copy-start | bytes 196612
  72.9 118.2 %collective-permute-start.1 = (bf16[128,128]{1,0:T(8,128)(2,1)}, bf16[128,128]{1,0:T(8,128)(2,1)}, u32[]{:S(2)}, u32[]{:S(2)}) collective-permute-start(bf16[128,128]{1,0:T(8,128)(2,1)} %slice.64), channel_id=1, source_target_pairs={{0,8},{8,16},{16,24},{1,9},{9,17},{17,25},{2,10},{10,18},{18,26},{... | collective-permute-start | bytes 98312 | tf_op jit(solution)/shard_map/ppermute | solution.py:41
  176.6 1.3 copy-start.8
  178.0 0.7 copy-start.3
  178.1 0.8 copy-start.1
  178.8 7.6 %copy-start.19 = (f32[256]{0:T(256)S(1)}, f32[256]{0:T(256)}, u32[]{:S(2)}) copy-start(f32[256]{0:T(256)} %copy-done.18) | copy-start | bytes 3076
  178.8 7.6 %copy-start.21 = (f32[2048]{0:T(1024)S(1)}, f32[2048]{0:T(1024)}, u32[]{:S(2)}) copy-start(f32[2048]{0:T(1024)} %param.19) | copy-start | bytes 24580
  185.6 2.7 copy-start.11
  186.4 104.1 %all-gather.24.cloned.1.call-start = ((), (), s32[]{:S(2)}) async-start(), calls=%async_computation.9 | async-start | bytes 2621440 | tf_op jit(solution)/shard_map/all_gather | solution.py:209
  188.3 31.2 %copy-start.6 = (bf16[1,256,2048]{2,1,0:T(8,128)(2,1)S(1)}, bf16[1,256,2048]{2,1,0:T(8,128)(2,1)}, u32[]{:S(2)}) copy-start(bf16[1,256,2048]{2,1,0:T(8,128)(2,1)} %all-gather.20.cloned.1.call-done) | copy-start | bytes 3145732
  188.6 4.3 %collective-permute-start = (bf16[128,128]{1,0:T(8,128)(2,1)S(1)}, bf16[128,128]{1,0:T(8,128)(2,1)S(1)}, u32[]{:S(2)}, u32[]{:S(2)}) collective-permute-start(bf16[128,128]{1,0:T(8,128)(2,1)S(1)} %slice.63), channel_id=1, source_target_pairs={{0,8},{8,16},{16,24},{1,9},{9,17},{17,25},{2,10},{10,18},{18,26},{... | collective-permute-start | bytes 98312 | tf_op jit(solution)/shard_map/ppermute | solution.py:41
  194.9 27.2 %copy-start.14 = (pred[2,128,256]{1,2,0:T(8,128)(4,1)S(1)}, pred[2,128,256]{1,2,0:T(8,128)(4,1)}, u32[]{:S(2)}) copy-start(pred[2,128,256]{1,2,0:T(8,128)(4,1)} %broadcast_and_fusion) | copy-start | bytes 196612
  221.8 1.0 copy-start.17
  248.9 4.6 %copy-start.2 = (f32[256,2,128]{2,0,1:T(8,128)S(1)}, f32[256,2,128]{2,0,1:T(8,128)}, u32[]{:S(2)}) copy-start(f32[256,2,128]{2,0,1:T(8,128)} %copy-done.1) | copy-start | bytes 786436
  248.9 4.6 %copy-start.4 = (f32[256,2,128]{2,0,1:T(8,128)S(1)}, f32[256,2,128]{2,0,1:T(8,128)}, u32[]{:S(2)}) copy-start(f32[256,2,128]{2,0,1:T(8,128)} %copy-done.3) | copy-start | bytes 786436
  248.9 4.6 %copy-start.9 = (f32[1,2,256,256]{3,2,1,0:T(8,128)S(1)}, f32[1,2,256,256]{3,2,1,0:T(8,128)}, u32[]{:S(2)}) copy-start(f32[1,2,256,256]{3,2,1,0:T(8,128)} %param.27) | copy-start | bytes 1572868
  253.5 1.3 copy-start.16
  255.9 65.2 %reduce-scatter.2.cloned.1.call-start = ((), (), s32[]{:S(2)}) async-start(), calls=%async_computation.6 | async-start | bytes 1572864 | tf_op jit(solution)/shard_map/reduce_scatter | solution.py:218
  293.3 1.0 copy-start.7
Sparse Core Ops, SparseCore 0:
  8.9 11.7 all-gather.19
  22.3 58.6 all-gather.11
  82.5 45.0 all-gather.15
  129.1 44.4 all-gather.13
  175.0 44.4 all-gather.17
  220.9 27.9 all-gather.21
  256.0 34.4 all-gather.23
  313.2 7.8 reduce-scatter.1
where the time goes:
time: 331 us; the launch traced here: 330 us
  waiting for transfers between devices  188 us (57%)
  blocking collectives  69.8 us (21%)
  matrix products  23 us (7%)
  local copies, waits for them, and re-layouts  16.4 us (5%)
  between operations  14.8 us (4%)
  other arithmetic  12.8 us (4%)
  starting transfers between devices  5.19 us (2%)
    all_gather x1, waiting for transfers between devices, shards(): lax.all_gather(weights[0], 'sp', axis=0, tiled=True)  44 us
    all_gather x1, waiting for transfers between devices, shards(): lax.all_gather(weights[2], 'sp', axis=0, tiled=True)  42.1 us
    all_gather x1, waiting for transfers between devices, shards(): piece = lax.all_gather(joined, 'fs', axis=0, tiled=True)  34.5 us
    all_gather x1, waiting for transfers between devices, carried_in(): lax.all_gather(part.astype(kind), axis)  25.1 us
    all_gather x1, waiting for transfers between devices, shards(): lax.all_gather(weights[3], 'sp', axis=0, tiled=True)  24.5 us
    all_gather x1, blocking collectives, shards(): lax.all_gather(weights[5], 'sp', axis=0, tiled=True)  21.2 us
    all_gather x1, blocking collectives, shards(): lax.all_gather(weights[4], 'sp', axis=0, tiled=True)  18.4 us
    all_to_all x1, blocking collectives, shards(): lax.all_to_all(partial_rows, 'fs', split_axis=0, concat_axis=2, tiled=True)  16.7 us
  transfers between devices with their start and end apart: 10, of which 8 were waited for; matrix products, arithmetic and copies ran while one was open for 11% of the time, Pallas kernels for 0%

commit v1 on v0

--- a/solution.py
+++ b/solution.py
@@ -10,6 +10,18 @@
 BLOCK = 128
 epsilon = 1e-06
 exact_result = lax.Precision.HIGHEST
+
+
+def exchange_directly(x, axis, split, join):
+    ways, here = (lax.axis_size(axis), lax.axis_index(axis))
+    width = x.shape[split] // ways
+    turned = jnp.roll(x, -here * width, axis=split)
+    got = [lax.slice_in_dim(turned, 0, width, axis=split)]
+    for far in range(1, ways):
+        sent = lax.slice_in_dim(turned, far * width, (far + 1) * width, axis=split)
+        got.append(lax.ppermute(sent, axis, [(d, (d + far) % ways) for d in range(ways)]))
+    line = jnp.concatenate(got[::-1], axis=join)
+    return jnp.roll(line, (here + 1) * got[0].shape[join], axis=join)
 
 
 def carried_in(array, axis, combine, identity):
@@ -214,7 +226,7 @@
         "srh,hd->srd", piece[:, :, ret_width:], att_out, preferred_element_type=jnp.float32
     )
     partial_rows = product.astype(jnp.bfloat16)
-    regrouped = lax.all_to_all(partial_rows, "fs", split_axis=0, concat_axis=2, tiled=True)
+    regrouped = exchange_directly(partial_rows, "fs", 0, 2)
     mixed = lax.psum_scatter(
         regrouped[0].astype(jnp.float32).astype(jnp.bfloat16), "tp", scatter_dimension=1, tiled=True
     )

time: 331 us -> 328 us (level)
  blocking collectives: 69.8 us -> 53 us
  waiting for transfers between devices: 188 us -> 200 us
  starting transfers between devices: 5.19 us -> 8.77 us
    all_to_all x1 -> x0, blocking collectives: 16.7 us -> none  [shards(): lax.all_to_all(partial_rows, 'fs', split_axis=0, concat_axis=2, tiled=True)]
    ppermute x0 -> x3, waiting for transfers between devices: none -> 11.2 us  [exchange_directly(): lax.ppermute(sent, axis, [(d, (d + far) % ways) for d in range(ways)])]
    ppermute x0 -> x3, starting transfers between devices: none -> 3.54 us  [exchange_directly(): lax.ppermute(sent, axis, [(d, (d + far) % ways) for d in range(ways)])]
  transfers between devices with their start and end apart: 10 -> 13, of which waited for: 8 -> 10; matrix products, arithmetic and copies ran while one was open for 11% -> 11% of each run, Pallas kernels for 0% -> 0%
where the time goes in v1:
time: 328 us; the launch traced here: 327 us
  waiting for transfers between devices  200 us (61%)
  blocking collectives  53 us (16%)
  matrix products  22.9 us (7%)
  between operations  14.8 us (5%)
  local copies, waits for them, and re-layouts  14.4 us (4%)
  other arithmetic  13.2 us (4%)
  starting transfers between devices  8.77 us (3%)
    all_gather x1, waiting for transfers between devices, shards(): lax.all_gather(weights[0], 'sp', axis=0, tiled=True)  44 us
    all_gather x1, waiting for transfers between devices, shards(): lax.all_gather(weights[2], 'sp', axis=0, tiled=True)  42.1 us
    all_gather x1, waiting for transfers between devices, shards(): piece = lax.all_gather(joined, 'fs', axis=0, tiled=True)  34.5 us
    all_gather x1, waiting for transfers between devices, carried_in(): lax.all_gather(part.astype(kind), axis)  25.1 us
    all_gather x1, waiting for transfers between devices, shards(): lax.all_gather(weights[3], 'sp', axis=0, tiled=True)  24.6 us
    all_gather x1, blocking collectives, shards(): lax.all_gather(weights[5], 'sp', axis=0, tiled=True)  21.1 us
    all_gather x1, blocking collectives, shards(): lax.all_gather(weights[4], 'sp', axis=0, tiled=True)  18.3 us
    dot_general x6, matrix products, shards(): jnp.dot(normed, piece, preferred_element_type=jnp.float32)  13.6 us
  transfers between devices with their start and end apart: 13, of which 10 were waited for; matrix products, arithmetic and copies ran while one was open for 11% of the time, Pallas kernels for 0%

profile of v1, /device:TPU:0, one launch (start us, length us, event | category | flops | bytes accessed | tf_op | source)
XLA Modules:
  0.0 326.9 jit_solution(15120475782086089852)
XLA Ops:
  7.3 0.7 all-gather.12.cloned.1.call-update
  12.8 13.6 %all-reduce = bf16[8]{0:T(256)(128)(2,1)S(1)} all-reduce(bf16[8]{0:T(256)(128)(2,1)S(1)} %dynamic-update-slice), channel_id=3, replica_groups=mesh['sp'=4,'fs'=4,'tp'=2] {'sp'}, use_global_device_ids=true, to_apply=%add | all-reduce | flops 8 | bytes 32
  26.5 18.3 %all_gather.42 = bf16[2048,128]{1,0:T(8,128)(2,1)S(1)} all-gather(bf16[512,128]{1,0:T(8,128)(2,1)S(1)} %copy-done.12), channel_id=1, replica_groups=mesh['sp'=4,'fs'=4,'tp'=2] {'sp'}, dimensions={0}, use_global_device_ids=true | all-gather | bytes 655360 | tf_op jit(solution)/shard_map/all_gather | solution.py:139
  45.6 21.1 %all_gather.41 = bf16[2048,128]{1,0:T(8,128)(2,1)} all-gather(bf16[512,128]{1,0:T(8,128)(2,1)S(1)} %copy-done.13), channel_id=1, replica_groups=mesh['sp'=4,'fs'=4,'tp'=2] {'sp'}, dimensions={0}, use_global_device_ids=true | all-gather | bytes 655360 | tf_op jit(solution)/shard_map/all_gather | solution.py:140
  66.7 1.2 multiply_cosine_fusion
  67.9 0.8 broadcast_and_fusion
  68.7 1.6 fusion.25
  70.3 1.7 convolution_convert_fusion.5
  72.7 2.7 collective-permute-start.1
  75.4 5.5 %all-gather.12.cloned.1.call-done = bf16[2048,512]{1,0:T(8,128)(2,1)} async-done(((bf16[512,512]{1,0:T(8,128)(2,1)}), bf16[2048,512]{1,0:T(8,128)(2,1)}) %all-gather.12.cloned.1.call-update) | async-done | bytes 2097168 | tf_op jit(solution)/shard_map/all_gather | solution.py:136
  80.8 2.3 fusion.31
  83.5 44.0 %all-gather.16.cloned.1.call-done = bf16[2048,512]{1,0:T(8,128)(2,1)} async-done(((bf16[512,512]{1,0:T(8,128)(2,1)}), bf16[2048,512]{1,0:T(8,128)(2,1)}) %all-gather.16.cloned.1.call-update) | async-done | bytes 2097168 | tf_op jit(solution)/shard_map/all_gather | solution.py:135
  127.5 2.7 fusion.33
  130.2 1.1 reshape.298
  131.4 42.1 %all-gather.14.cloned.1.call-done = bf16[2048,512]{1,0:T(8,128)(2,1)} async-done(((bf16[512,512]{1,0:T(8,128)(2,1)}), bf16[2048,512]{1,0:T(8,128)(2,1)}) %all-gather.14.cloned.1.call-update) | async-done | bytes 2097168 | tf_op jit(solution)/shard_map/all_gather | solution.py:137
  173.5 2.7 fusion.32
  176.5 1.3 fusion.67
  178.8 6.7 %while.29 = (s32[]{:T(128)}, f32[2,256,256]{2,1,0:T(8,128)S(1)}, f32[2,2,128,256]{3,2,1,0:T(8,128)}, f32[2,2,128]{2,1,0:T(2,128)S(1)}, f32[2,2,128,256]{3,2,0,1:...) while((s32[]{:T(128)}, f32[2,256,256]{2,1,0:T(8,128)S(1)}, ...), condition=%wide.region_3.4_spmd.clone, body=%wide.region_1.3_spmd.clone.sunk | while | flops 604880896 | bytes 4242084 | solution.py:160
  180.1 1.2 fusion.97
  181.3 0.8 convolution_add_fusion.3
  183.5 1.2 fusion.97
  184.7 0.8 convolution_add_fusion.3
  185.5 0.7 convert_element_type.102
  186.3 1.9 convolution_convert_fusion.6
  188.6 2.2 collective-permute-start
  190.9 0.8 pad_maximum_fusion.2
  191.9 1.0 collective-permute-done
  193.1 1.3 copy.63
  194.8 24.6 %all-gather.18.cloned.1.call-done = bf16[2048,512]{1,0:T(8,128)(2,1)} async-done(((bf16[512,512]{1,0:T(8,128)(2,1)}), bf16[2048,512]{1,0:T(8,128)(2,1)}) %all-gather.18.cloned.1.call-update) | async-done | bytes 2097168 | tf_op jit(solution)/shard_map/all_gather | solution.py:138
  219.4 2.3 convolution_convert_fusion.1
  223.7 25.1 %all-gather.22.cloned.1.call-done = bf16[8,256,256]{2,1,0:T(8,128)(2,1)} async-done(((bf16[2,256,256]{2,1,0:T(8,128)(2,1)}), bf16[8,256,256]{2,1,0:T(8,128)(2,1)}) %all-gather.22.cloned.1.call-update) | async-done | bytes 1048592 | tf_op jit(solution)/shard_map/all_gather | solution.py:30
  248.8 4.6 %while.30 = (s32[]{:T(128)}, f32[2]{0:T(128)S(1)}, f32[2,256,256]{2,1,0:T(8,128)S(1)}, s32[]{:T(128)}, bf16[4,2]{1,0:T(4,128)(2,1)S(1)}, /*index=5*/bf16[4,2,256,256]{3,2,1,0:T(8,128)(2,1)}, s32[]{:T(128)}, s32[]{:T(128)}) while((s32[]{:T(128)}, f32[2]{0:T(128)S(1)}, f32[2,256,256]{2,1,0:T(8,128)S(1)}, s32[]{:T(128)}, ...), condition=%wide.region_7.8_spmd.clone, body=%wide.region_6.7_spmd.clone.sunk | while | flops 655372 | bytes 1310871 | solution.py:47
  248.8 1.2 fusion.98
  250.0 1.1 fusion.98
  251.2 1.1 fusion.98
  252.3 1.1 fusion.98
  253.5 1.2 fusion.69
  254.9 0.8 pad_maximum_fusion.1
  255.9 34.5 %all-gather.24.cloned.1.call-done = bf16[1024,1024]{0,1:T(8,128)(2,1)} async-done(((bf16[256,1024]{0,1:T(8,128)(2,1)}), bf16[1024,1024]{0,1:T(8,128)(2,1)}) %all-gather.24.cloned.1.call-update) | async-done | bytes 2097168 | tf_op jit(solution)/shard_map/all_gather | solution.py:221
  290.4 2.9 copy.79
  293.2 0.7 fusion.37
  294.3 0.7 add_convert_fusion
  295.5 1.5 collective-permute-start.2
  297.0 1.5 collective-permute-start.3
  299.0 5.7 %collective-permute-done.2 = bf16[1,256,512]{2,1,0:T(8,128)(2,1)S(1)} collective-permute-done((bf16[1,256,512]{2,1,0:T(8,128)(2,1)S(1)}, bf16[1,256,512]{2,1,0:T(8,128)(2,1)S(1)}, u32[]{:S(2)}, u32[]{:S(2)}) %collective-permute-start.2) | collective-permute-done | bytes 262176 | tf_op jit(solution)/shard_map/ppermute | solution.py:22
  304.7 5.5 %collective-permute-done.3 = bf16[1,256,512]{2,1,0:T(8,128)(2,1)S(1)} collective-permute-done((bf16[1,256,512]{2,1,0:T(8,128)(2,1)S(1)}, bf16[1,256,512]{2,1,0:T(8,128)(2,1)S(1)}, u32[]{:S(2)}, u32[]{:S(2)}) %collective-permute-start.3) | collective-permute-done | bytes 262176 | tf_op jit(solution)/shard_map/ppermute | solution.py:22
  310.5 1.1 dynamic-slice_bitcast_fusion
  311.6 8.5 %reduce-scatter.2.cloned.1.call-done = bf16[256,1024]{1,0:T(8,128)(2,1)} async-done(((bf16[256,2048]{1,0:T(8,128)(2,1)}), bf16[256,1024]{1,0:T(8,128)(2,1)}) %reduce-scatter.2.cloned.1.call-update) | async-done | bytes 524304 | tf_op jit(solution)/shard_map/reduce_scatter | solution.py:230
  (152 shorter events, 15.8 us)
Async XLA Ops:
  6.5 286.7 %copy-start = (bf16[512,512]{1,0:T(8,128)(2,1)S(1)}, bf16[512,512]{1,0:T(8,128)(2,1)}, u32[]{:S(2)}) copy-start(bf16[512,512]{1,0:T(8,128)(2,1)} %param.30) | copy-start | bytes 1572868
  6.5 4.8 %copy-start.23 = (u32[32]{0:T(128)S(1)}, u32[32]{0:T(128)}, u32[]{:S(2)}) copy-start(u32[32]{0:T(128)} %constant.141) | copy-start | bytes 388
  6.5 3.5 %copy-start.15 = (f32[1,2,256]{2,1,0:T(2,128)S(1)}, f32[1,2,256]{2,1,0:T(2,128)}, u32[]{:S(2)}) copy-start(f32[1,2,256]{2,1,0:T(2,128)} %param.26) | copy-start | bytes 6148
  6.5 20.0 %copy-start.12 = (bf16[512,128]{1,0:T(8,128)(2,1)S(1)}, bf16[512,128]{1,0:T(8,128)(2,1)}, u32[]{:S(2)}) copy-start(bf16[512,128]{1,0:T(8,128)(2,1)} %param.24) | copy-start | bytes 393220
  6.5 38.4 %copy-start.22 = (f32[8]{0:T(128)S(1)}, f32[8]{0:T(128)}, u32[]{:S(2)}) copy-start(f32[8]{0:T(128)} %param.29) | copy-start | bytes 100
  6.5 39.1 %copy-start.13 = (bf16[512,128]{1,0:T(8,128)(2,1)S(1)}, bf16[512,128]{1,0:T(8,128)(2,1)}, u32[]{:S(2)}) copy-start(bf16[512,128]{1,0:T(8,128)(2,1)} %param.25) | copy-start | bytes 393220
  6.6 62.1 %all-gather.20.cloned.1.call-start = ((), (), s32[]{:S(2)}) async-start(), calls=%async_computation.6 | async-start | bytes 1572864 | tf_op jit(solution)/shard_map/all_gather | solution.py:123
  7.3 73.5 %all-gather.12.cloned.1.call-start = ((), (), s32[]{:S(2)}) async-start(), calls=%async_computation.1 | async-start | bytes 2621440 | tf_op jit(solution)/shard_map/all_gather | solution.py:136
  8.0 62.3 %copy-start.20 = (f32[2048]{0:T(1024)S(1)}, f32[2048]{0:T(1024)}, u32[]{:S(2)}) copy-start(f32[2048]{0:T(1024)} %param.19) | copy-start | bytes 24580
  8.1 119.5 %all-gather.16.cloned.1.call-start = ((), (), s32[]{:S(2)}) async-start(), calls=%async_computation.3 | async-start | bytes 2621440 | tf_op jit(solution)/shard_map/all_gather | solution.py:135
  8.8 164.7 %all-gather.14.cloned.1.call-start = ((), (), s32[]{:S(2)}) async-start(), calls=%async_computation.2 | async-start | bytes 2621440 | tf_op jit(solution)/shard_map/all_gather | solution.py:137
  9.4 210.0 %all-gather.18.cloned.1.call-start = ((), (), s32[]{:S(2)}) async-start(), calls=%async_computation.4 | async-start | bytes 2621440 | tf_op jit(solution)/shard_map/all_gather | solution.py:138
  10.0 238.8 %all-gather.22.cloned.1.call-start = ((), (), s32[]{:S(2)}) async-start(), calls=%async_computation.7 | async-start | bytes 1310720 | tf_op jit(solution)/shard_map/all_gather | solution.py:30
  68.7 12.1 %copy-start.5 = (bf16[1,256,2048]{2,1,0:T(8,128)(2,1)S(1)}, bf16[1,256,2048]{2,1,0:T(8,128)(2,1)}, u32[]{:S(2)}) copy-start(bf16[1,256,2048]{2,1,0:T(8,128)(2,1)} %all-gather.20.cloned.1.call-done) | copy-start | bytes 3145732
  70.3 103.1 %copy-start.18 = (f32[256]{0:T(256)}, f32[256]{0:T(256)S(1)}, u32[]{:S(2)}) copy-start(f32[256]{0:T(256)S(1)} %add_rsqrt_fusion.1) | copy-start | bytes 3076
  72.0 11.1 %copy-start.10 = (bf16[256,128]{1,0:T(8,128)(2,1)}, bf16[256,128]{1,0:T(8,128)(2,1)S(1)}, u32[]{:S(2)}) copy-start(bf16[256,128]{1,0:T(8,128)(2,1)S(1)} %convolution_convert_fusion.5) | copy-start | bytes 196612
  72.7 118.2 %collective-permute-start.1 = (bf16[128,128]{1,0:T(8,128)(2,1)}, bf16[128,128]{1,0:T(8,128)(2,1)}, u32[]{:S(2)}, u32[]{:S(2)}) collective-permute-start(bf16[128,128]{1,0:T(8,128)(2,1)} %slice.80), channel_id=1, source_target_pairs={{0,8},{8,16},{16,24},{1,9},{9,17},{17,25},{2,10},{10,18},{18,26},{... | collective-permute-start | bytes 98312 | tf_op jit(solution)/shard_map/ppermute | solution.py:53
  176.5 1.3 copy-start.8
  177.9 0.7 copy-start.3
  178.0 0.8 copy-start.1
  178.7 7.6 %copy-start.19 = (f32[256]{0:T(256)S(1)}, f32[256]{0:T(256)}, u32[]{:S(2)}) copy-start(f32[256]{0:T(256)} %copy-done.18) | copy-start | bytes 3076
  178.7 7.6 %copy-start.21 = (f32[2048]{0:T(1024)S(1)}, f32[2048]{0:T(1024)}, u32[]{:S(2)}) copy-start(f32[2048]{0:T(1024)} %param.19) | copy-start | bytes 24580
  185.5 2.7 copy-start.11
  186.3 104.1 %all-gather.24.cloned.1.call-start = ((), (), s32[]{:S(2)}) async-start(), calls=%async_computation.8 | async-start | bytes 2621440 | tf_op jit(solution)/shard_map/all_gather | solution.py:221
  188.2 31.2 %copy-start.6 = (bf16[1,256,2048]{2,1,0:T(8,128)(2,1)S(1)}, bf16[1,256,2048]{2,1,0:T(8,128)(2,1)}, u32[]{:S(2)}) copy-start(bf16[1,256,2048]{2,1,0:T(8,128)(2,1)} %all-gather.20.cloned.1.call-done) | copy-start | bytes 3145732
  188.6 4.3 %collective-permute-start = (bf16[128,128]{1,0:T(8,128)(2,1)S(1)}, bf16[128,128]{1,0:T(8,128)(2,1)S(1)}, u32[]{:S(2)}, u32[]{:S(2)}) collective-permute-start(bf16[128,128]{1,0:T(8,128)(2,1)S(1)} %slice.79), channel_id=1, source_target_pairs={{0,8},{8,16},{16,24},{1,9},{9,17},{17,25},{2,10},{10,18},{18,26},{... | collective-permute-start | bytes 98312 | tf_op jit(solution)/shard_map/ppermute | solution.py:53
  194.8 27.2 %copy-start.14 = (pred[2,128,256]{1,2,0:T(8,128)(4,1)S(1)}, pred[2,128,256]{1,2,0:T(8,128)(4,1)}, u32[]{:S(2)}) copy-start(pred[2,128,256]{1,2,0:T(8,128)(4,1)} %broadcast_and_fusion) | copy-start | bytes 196612
  221.7 1.0 copy-start.17
  248.8 4.6 %copy-start.2 = (f32[256,2,128]{2,0,1:T(8,128)S(1)}, f32[256,2,128]{2,0,1:T(8,128)}, u32[]{:S(2)}) copy-start(f32[256,2,128]{2,0,1:T(8,128)} %copy-done.1) | copy-start | bytes 786436
  248.8 4.6 %copy-start.4 = (f32[256,2,128]{2,0,1:T(8,128)S(1)}, f32[256,2,128]{2,0,1:T(8,128)}, u32[]{:S(2)}) copy-start(f32[256,2,128]{2,0,1:T(8,128)} %copy-done.3) | copy-start | bytes 786436
  248.8 4.6 %copy-start.9 = (f32[1,2,256,256]{3,2,1,0:T(8,128)S(1)}, f32[1,2,256,256]{3,2,1,0:T(8,128)}, u32[]{:S(2)}) copy-start(f32[1,2,256,256]{3,2,1,0:T(8,128)} %param.27) | copy-start | bytes 1572868
  253.5 1.3 copy-start.16
  255.8 64.3 %reduce-scatter.2.cloned.1.call-start = ((), (), s32[]{:S(2)}) async-start(), calls=%async_computation.5 | async-start | bytes 1572864 | tf_op jit(solution)/shard_map/reduce_scatter | solution.py:230
  293.2 1.0 copy-start.7
  295.5 9.2 %collective-permute-start.2 = (bf16[1,256,512]{2,1,0:T(8,128)(2,1)S(1)}, bf16[1,256,512]{2,1,0:T(8,128)(2,1)S(1)}, u32[]{:S(2)}, u32[]{:S(2)}) collective-permute-start(bf16[1,256,512]{2,1,0:T(8,128)(2,1)S(1)} %get-tuple-element.248), channel_id=1, source_target_pairs={{0,6},{2,0},{4,2},{6,4},{1,7},{3,1},{5,3},{7,5},{8,14},{10,8},{12,... | collective-permute-start | bytes 786440 | tf_op jit(solution)/shard_map/ppermute | solution.py:22
  297.0 13.2 %collective-permute-start.3 = (bf16[1,256,512]{2,1,0:T(8,128)(2,1)S(1)}, bf16[1,256,512]{2,1,0:T(8,128)(2,1)S(1)}, u32[]{:S(2)}, u32[]{:S(2)}) collective-permute-start(bf16[1,256,512]{2,1,0:T(8,128)(2,1)S(1)} %get-tuple-element.247), channel_id=1, source_target_pairs={{0,4},{2,6},{4,0},{6,2},{1,5},{3,7},{5,1},{7,3},{8,12},{10,14},{12... | collective-permute-start | bytes 786440 | tf_op jit(solution)/shard_map/ppermute | solution.py:22
  298.4 11.8 %collective-permute-start.4 = (bf16[1,256,512]{2,1,0:T(8,128)(2,1)S(1)}, bf16[1,256,512]{2,1,0:T(8,128)(2,1)S(1)}, u32[]{:S(2)}, u32[]{:S(2)}) collective-permute-start(bf16[1,256,512]{2,1,0:T(8,128)(2,1)S(1)} %get-tuple-element.246), channel_id=1, source_target_pairs={{0,2},{2,4},{4,6},{6,0},{1,3},{3,5},{5,7},{7,1},{8,10},{10,12},{12... | collective-permute-start | bytes 786440 | tf_op jit(solution)/shard_map/ppermute | solution.py:22
Sparse Core Ops, SparseCore 0:
  8.9 11.7 all-gather.19
  22.3 58.5 all-gather.11
  82.4 45.0 all-gather.15
  129.0 44.4 all-gather.13
  174.9 44.4 all-gather.17
  220.8 27.9 all-gather.21
  255.9 34.4 all-gather.23
  311.7 8.3 reduce-scatter.1
